TPU v7x, 32 devices: a whole 2x2x4 slice. The times are simulated.
32 devices in a mesh: tp: 8 (over z, y), dp: 4 (over x, core).
Axes of the slice: x: 2, y: 2, z: 4, core: 2. Of those that a mesh axis runs over, the one named last changes fastest.
Arguments:
- incoming_token: bfloat16 [128, 4096], P(None, 'dp'), may hold values from -60 to 60
- input_norm_gain: float32 [2, 4096], P(None, 'dp'), may hold values from 0.1 to 1.9
- receptance_weight: bfloat16 [2, 4096, 8192], P(None, 'dp', 'tp'), may hold values from -0.09375 to 0.09375
- key_weight: bfloat16 [2, 4096, 8192], P(None, 'dp', 'tp'), may hold values from -0.09375 to 0.09375
- value_weight: bfloat16 [2, 4096, 8192], P(None, 'dp', 'tp'), may hold values from -0.09375 to 0.09375
- decay_weight: bfloat16 [2, 4096, 8192], P(None, 'dp', 'tp'), may hold values from -0.09375 to 0.09375
- learning_rate_weight: bfloat16 [2, 4096, 8192], P(None, 'dp', 'tp'), may hold values from -0.09375 to 0.09375
- gate_weight: bfloat16 [2, 4096, 8192], P(None, 'dp', 'tp'), may hold values from -0.09375 to 0.09375
- channel_decay_floor: float32 [2, 8192], P(None, 'tp'), may hold values from -5 to 2
- direct_token_weight: float32 [2, 8192], P(None, 'tp'), may hold values from -0.6 to 0.6
- head_norm_gain: float32 [2, 8192], P(None, 'tp'), may hold values from 0.1 to 1.9
- output_weight: bfloat16 [2, 8192, 4096], P(None, 'tp', 'dp'), may hold values from -0.0625 to 0.0625
- incoming_state: float32 [2, 128, 128, 64, 64], P(None, 'dp', 'tp'), may hold values from -6 to 6
Outputs:
- hidden_out: bfloat16 [128, 4096], P(None, 'dp')
- state_out: float32 [2, 128, 128, 64, 64], P(None, 'dp', 'tp')
All inputs are finite; a program needn't handle non-finite values.
Results may differ from a plain program's by a relative error of at most 0.0053.
Values may be sent and summed in bfloat16 or wider, within the bound.
A program may use at most 192 MiB of HBM per device.

v0:
```python
import jax
import jax.numpy as jnp
from jax import lax
from jax.sharding import PartitionSpec as P

D = 4096
HEAD_CHANNELS = 64


def recurrent_mix_heads(
    projected_output, earlier_state, channel_decay_floor, direct_token_weight, head_norm_gain
):
    step_count = projected_output.shape[0]
    local_heads = channel_decay_floor.shape[0] // HEAD_CHANNELS
    sections = projected_output.reshape(step_count, 6, local_heads, HEAD_CHANNELS)
    receptance_rows, keyvec, value_vector, pre_decay, pre_rate, pre_gate = [
        sections[:, part_index] for part_index in range(6)
    ]
    decay_pre = channel_decay_floor.reshape(local_heads, HEAD_CHANNELS) + pre_decay
    decay_factor = jnp.exp(-jnp.exp(-jax.nn.softplus(-decay_pre) - 0.5))
    learn_rate = jax.nn.sigmoid(pre_rate)
    output_gate_value = jax.nn.sigmoid(pre_gate)
    unit_key = keyvec * lax.rsqrt(jnp.sum(keyvec * keyvec, axis=-1, keepdims=True) + 1e-06)
    rescaled_key = keyvec * learn_rate
    removed = -jnp.einsum("shvk,shk->shv", earlier_state, unit_key, precision=lax.Precision.HIGHEST)
    refreshed_state = (
        earlier_state * decay_factor[:, :, None, :]
        + removed[..., None] * (unit_key * learn_rate)[:, :, None, :]
        + value_vector[..., None] * rescaled_key[:, :, None, :]
    )
    readout = jnp.einsum(
        "shvk,shk->shv", refreshed_state, receptance_rows, precision=lax.Precision.HIGHEST
    )
    group_mean = jnp.mean(readout, axis=-1, keepdims=True)
    group_var = jnp.mean(jnp.square(readout - group_mean), axis=-1, keepdims=True)
    normalized_input = (
        (readout - group_mean)
        * lax.rsqrt(group_var + 0.00064)
        * head_norm_gain.reshape(local_heads, HEAD_CHANNELS)
    )
    direct_token_term = (
        jnp.sum(
            receptance_rows
            * rescaled_key
            * direct_token_weight.reshape(local_heads, HEAD_CHANNELS),
            axis=-1,
            keepdims=True,
        )
        * value_vector
    )
    mixer_output = (
        ((normalized_input + direct_token_term) * output_gate_value)
        .reshape(step_count, local_heads * HEAD_CHANNELS)
        .astype(jnp.bfloat16)
    )
    return (mixer_output, refreshed_state)


def per_device(
    incoming_token,
    input_norm_gain,
    receptance_weight,
    key_weight,
    value_weight,
    decay_weight,
    learning_rate_weight,
    gate_weight,
    channel_decay_floor,
    direct_token_weight,
    head_norm_gain,
    output_weight,
    incoming_state,
):
    hidden = incoming_token
    new_states = []
    for block_index in range(2):
        hidden_wide = hidden.astype(jnp.float32)
        partial_squares = jnp.sum(hidden_wide * hidden_wide, axis=1)
        scaled_in = (hidden_wide * input_norm_gain[block_index]).astype(jnp.bfloat16)
        matrices = (
            receptance_weight[block_index],
            key_weight[block_index],
            value_weight[block_index],
            decay_weight[block_index],
            learning_rate_weight[block_index],
            gate_weight[block_index],
        )
        partial_terms = jnp.concatenate(
            [jnp.dot(scaled_in, matrix, preferred_element_type=jnp.float32) for matrix in matrices],
            axis=1,
        )
        summed, own_squares = (
            lax.psum_scatter(partial_terms, "dp", scatter_dimension=0, tiled=True),
            lax.psum_scatter(partial_squares, "dp", scatter_dimension=0, tiled=True),
        )
        projected_output = summed * lax.rsqrt(own_squares[:, None] / D + 1e-06)
        mixer_output, refreshed_state = recurrent_mix_heads(
            projected_output,
            incoming_state[block_index],
            channel_decay_floor[block_index],
            direct_token_weight[block_index],
            head_norm_gain[block_index],
        )
        new_states.append(refreshed_state)
        out_matrix = output_weight[block_index]
        branch = jnp.dot(
            lax.all_gather(mixer_output, "dp", axis=0, tiled=True),
            out_matrix,
            preferred_element_type=jnp.float32,
        )
        hidden = (hidden_wide + lax.psum(branch, "tp")).astype(jnp.bfloat16)
    return (hidden, jnp.stack(new_states))


def solution(mesh):
    return jax.shard_map(
        per_device,
        mesh=mesh,
        in_specs=(
            P(None, "dp"),
            P(None, "dp"),
            P(None, "dp", "tp"),
            P(None, "dp", "tp"),
            P(None, "dp", "tp"),
            P(None, "dp", "tp"),
            P(None, "dp", "tp"),
            P(None, "dp", "tp"),
            P(None, "tp"),
            P(None, "tp"),
            P(None, "tp"),
            P(None, "tp", "dp"),
            P(None, "dp", "tp", None, None),
        ),
        out_specs=(P(None, "dp"), P(None, "dp", "tp", None, None)),
        check_vma=False,
    )
```

profile of v0, /device:TPU:0, one launch (start us, length us, event | category | flops | bytes accessed | tf_op | source)
XLA Modules:
  0.0 434.6 jit_solution(2424287610302264044)
XLA Ops:
  7.2 0.0 reduce-scatter.3.cloned.1.call-start
  7.2 0.9 fusion.186
  8.1 2.5 fusion.74
  10.7 2.3 fusion.77
  13.0 0.4 fusion.80
  13.4 0.4 fusion.83
  13.9 0.4 fusion.86
  14.4 2.0 fusion.89
  16.4 1.7 copy-done
  18.1 0.0 all-reduce.5.cloned.1.call-start
  18.2 0.6 dynamic-slice
  19.5 0.1 add.171
  19.6 0.1 mul.344
  19.7 0.1 mul.340
  19.7 0.1 fusion.119
  19.9 8.5 %all-reduce = f32[128]{0:T(128)S(1)} all-reduce(f32[128]{0:T(128)S(1)} %fusion.119), channel_id=3, replica_groups=mesh['tp'=8,'dp'=4] {'dp'}, use_global_device_ids=true, to_apply=%region_2.0.clone | all-reduce | flops 128 | bytes 1024
  28.4 0.1 fusion.179
  28.5 30.4 %reduce-scatter.3.cloned.1.call-done = f32[32,6144]{1,0:T(8,128)} async-done(((f32[128,6144]{1,0:T(8,128)}), f32[32,6144]{1,0:T(8,128)}) %reduce-scatter.3.cloned.1.call-update) | async-done | bytes 786448 | tf_op jit(solution)/shard_map/reduce_scatter | solution.py:93
  58.9 1.3 broadcast_multiply_fusion.1
  60.2 0.6 reshape.188
  60.9 0.3 fusion.129
  61.2 0.1 fusion.175
  61.3 28.7 %fusion.8 = f32[32,16,1,64]{3,2,1,0:T(1,128)S(1)} fusion(f32[32,16,64,1]{2,3,1,0:T(1,128)S(1)} %bitcast.229, f32[2,32,16,64,64]{4,3,2,1,0:T(8,128)} %param.25), kind=kOutput, calls=%fused_computation.9 | convolution fusion | flops 25165824 | bytes 17039360 | tf_op jit(solution)/shard_map/shvk,shk->shv/dot_general | solution.py:25
  90.1 33.4 %fusion.12 = f32[32,16,1,64]{3,2,1,0:T(1,128)S(1)} fusion(f32[32,16,64,1]{2,3,1,0:T(1,128)S(1)} %bitcast.237, f32[2,32,16,64,64]{4,3,2,1,0:T(8,128)} %param.25, f32[32,16,64]{2,1,0:T(8,128)S(1)} %get-tuple-element.23, f32[32,16,64]{2,1,0:T(8,128)S(1)} %get-tuple-element.25, f32[32,16,64]{2,1,0:T(8,128)S(1)} %get-tuple-element.12, ...), kind=kOutput, calls=%fused_computation.14 | convolution fusion | flops 35651584 | bytes 17694720 | tf_op jit(solution)/shard_map/shvk,shk->shv/dot_general | solution.py:31
  123.5 0.1 reduce_sum.92
  123.7 0.2 multiply_reduce_fusion.2
  124.0 1.0 fusion.117
  125.0 0.1 convert_element_type.33
  125.1 5.8 %all_gather.6 = bf16[128,1024]{1,0:T(8,128)(2,1)S(1)} all-gather(bf16[32,1024]{1,0:T(8,128)(2,1)S(1)} %convert_element_type.33), channel_id=1, replica_groups=mesh['tp'=8,'dp'=4] {'dp'}, dimensions={0}, use_global_device_ids=true | all-gather | bytes 327680 | tf_op jit(solution)/shard_map/all_gather | solution.py:107
  130.9 2.8 fusion.46
  133.8 0.0 reduce-scatter.5.cloned.1.call-start
  133.8 72.8 %all-reduce.5.cloned.1.call-done = f32[128,1024]{1,0:T(8,128)} async-done(((f32[128,1024]{1,0:T(8,128)}), f32[128,1024]{1,0:T(8,128)}) %all-reduce.5.cloned.1.call-update) | async-done | bytes 524304 | tf_op jit(solution)/shard_map/psum | solution.py:111
  206.6 1.4 fusion.122
  208.0 2.2 fusion.92
  210.2 0.4 fusion.95
  210.7 2.2 fusion.98
  212.9 0.4 fusion.101
  213.4 0.4 fusion.104
  213.9 0.6 copy-done.23
  214.4 0.4 fusion.107
  214.9 1.7 copy-done.1
  216.5 0.0 all-reduce.7.cloned.1.call-start
  216.6 0.1 add.184
  216.7 0.1 mul.376
  216.7 0.1 mul.372
  216.8 5.9 %all-reduce.1 = f32[128]{0:T(128)S(1)} all-reduce(f32[128]{0:T(128)S(1)} %get-tuple-element.10), channel_id=5, replica_groups=mesh['tp'=8,'dp'=4] {'dp'}, use_global_device_ids=true, to_apply=%region_10.11.clone | all-reduce | flops 128 | bytes 1024
  222.7 0.1 fusion.180
  222.7 31.0 %reduce-scatter.5.cloned.1.call-done = f32[32,6144]{1,0:T(8,128)} async-done(((f32[128,6144]{1,0:T(8,128)}), f32[32,6144]{1,0:T(8,128)}) %reduce-scatter.5.cloned.1.call-update) | async-done | bytes 786448 | tf_op jit(solution)/shard_map/reduce_scatter | solution.py:93
  253.8 1.3 broadcast_multiply_fusion
  255.0 0.6 reshape.189
  255.7 0.1 multiply_reduce_fusion.1
  255.9 0.3 fusion.134
  256.2 28.7 %fusion.2 = f32[32,16,1,64]{3,2,1,0:T(1,128)S(1)} fusion(f32[32,16,64,1]{2,3,1,0:T(1,128)S(1)} %bitcast.226, f32[2,32,16,64,64]{4,3,2,1,0:T(8,128)} %param.25), kind=kOutput, calls=%fused_computation.3 | convolution fusion | flops 25165824 | bytes 17039360 | tf_op jit(solution)/shard_map/shvk,shk->shv/dot_general | solution.py:25
  285.0 24.9 %multiply_add_fusion.1 = (f32[1,32,16,64,64]{4,3,2,1,0:T(8,128)}, f32[1,32,16,64,64]{4,3,2,1,0:T(8,128)}) fusion(f32[2,32,16,64,64]{4,3,2,1,0:T(8,128)} %param.25, f32[32,16,64]{2,1,0:T(8,128)S(1)} %copy-done.7, f32[32,16,64]{2,1,0:T(8,128)S(1)} %copy-done.3, f32[32,16,64]{2,1,0:T(8,128)S(1)} %copy-done.9, f32[32,16,64]{2,1,0:T(8,128)S(1)} %neg.97, ...), kind=kLoop, calls=%fused_computation.16 | loop fusion | flops 20971520 | bytes 34865152 | tf_op jit(solution)/shard_map/add | solution.py:27
  309.9 33.4 %fusion.6 = f32[32,16,1,64]{3,2,1,0:T(1,128)S(1)} fusion(f32[32,16,64,1]{2,3,1,0:T(1,128)S(1)} %bitcast.236, f32[2,32,16,64,64]{4,3,2,1,0:T(8,128)} %param.25, f32[32,16,64]{2,1,0:T(8,128)S(1)} %get-tuple-element.17, f32[32,16,64]{2,1,0:T(8,128)S(1)} %get-tuple-element.20, f32[32,16,64]{2,1,0:T(8,128)S(1)} %get-tuple-element.18, ...), kind=kOutput, calls=%fused_computation.8 | convolution fusion | flops 35651584 | bytes 17694720 | tf_op jit(solution)/shard_map/shvk,shk->shv/dot_general | solution.py:31
  343.2 0.1 reduce_sum.97
  343.4 0.2 multiply_reduce_fusion
  343.7 1.0 fusion.116
  344.7 0.1 convert_element_type.38
  344.8 5.8 %all_gather.7 = bf16[128,1024]{1,0:T(8,128)(2,1)S(1)} all-gather(bf16[32,1024]{1,0:T(8,128)(2,1)S(1)} %convert_element_type.38), channel_id=1, replica_groups=mesh['tp'=8,'dp'=4] {'dp'}, dimensions={0}, use_global_device_ids=true | all-gather | bytes 327680 | tf_op jit(solution)/shard_map/all_gather | solution.py:107
  350.6 2.8 fusion.32
  353.5 24.7 %pad_maximum_fusion = f32[2,32,16,64,64]{4,3,2,1,0:T(8,128)} fusion(f32[1,32,16,64,64]{4,3,2,1,0:T(8,128)} %get-tuple-element.15, f32[1,32,16,64,64]{4,3,2,1,0:T(8,128)} %get-tuple-element.14), kind=kLoop, calls=%fused_computation.2 | loop fusion | flops 4194304 | bytes 33554432 | tf_op jit(solution)/shard_map/stack | solution.py:112
  378.2 48.1 %all-reduce.7.cloned.1.call-done = f32[128,1024]{1,0:T(8,128)} async-done(((f32[128,1024]{1,0:T(8,128)}), f32[128,1024]{1,0:T(8,128)}) %all-reduce.7.cloned.1.call-update) | async-done | bytes 524304 | tf_op jit(solution)/shard_map/psum | solution.py:111
  426.3 1.8 fusion.123
  (63 shorter events, 0.4 us)
Async XLA Ops:
  7.2 5.8 %copy-start.10 = (bf16[128,1024]{1,0:T(8,128)(2,1)S(1)}, bf16[128,1024]{1,0:T(8,128)(2,1)}, u32[]{:S(2)}) copy-start(bf16[128,1024]{1,0:T(8,128)(2,1)} %param.13) | copy-start | bytes 786436
  7.2 51.7 %reduce-scatter.3.cloned.1.call-start = ((), (), s32[]{:S(2)}) async-start(), calls=%async_computation.2 | async-start | bytes 3932160 | tf_op jit(solution)/shard_map/reduce_scatter | solution.py:93
  7.2 5.7 %copy-start.18 = (bf16[2,1024,1024]{2,1,0:T(8,128)(2,1)S(1)}, bf16[2,1024,1024]{2,1,0:T(8,128)(2,1)}, u32[]{:S(2)}) copy-start(bf16[2,1024,1024]{2,1,0:T(8,128)(2,1)} %param.17) | copy-start | bytes 12582916
  8.1 5.3 %copy-start.19 = (bf16[2,1024,1024]{2,1,0:T(8,128)(2,1)S(1)}, bf16[2,1024,1024]{2,1,0:T(8,128)(2,1)}, u32[]{:S(2)}) copy-start(bf16[2,1024,1024]{2,1,0:T(8,128)(2,1)} %param.18) | copy-start | bytes 12582916
  10.7 3.2 copy-start.21
  13.9 4.3 copy-start.24
  13.9 5.5 %copy-start.14 = (f32[2,1024]{1,0:T(2,128)S(1)}, f32[2,1024]{1,0:T(2,128)}, u32[]{:S(2)}) copy-start(f32[2,1024]{1,0:T(2,128)} %param.21) | copy-start | bytes 24580
  13.9 5.6 %copy-start.15 = (f32[2,1024]{1,0:T(2,128)S(1)}, f32[2,1024]{1,0:T(2,128)}, u32[]{:S(2)}) copy-start(f32[2,1024]{1,0:T(2,128)} %param.22) | copy-start | bytes 24580
  13.9 5.6 %copy-start.16 = (f32[2,1024]{1,0:T(2,128)S(1)}, f32[2,1024]{1,0:T(2,128)}, u32[]{:S(2)}) copy-start(f32[2,1024]{1,0:T(2,128)} %param.23) | copy-start | bytes 24580
  16.4 1.7 copy-start
  18.1 188.5 %all-reduce.5.cloned.1.call-start = ((), (), s32[]{:S(2)}) async-start(), calls=%async_computation.3 | async-start | bytes 1048576 | tf_op jit(solution)/shard_map/psum | solution.py:111
  60.8 29.3 %copy-start.2 = (f32[32,16,64]{2,1,0:T(8,128)}, f32[32,16,64]{2,1,0:T(8,128)S(1)}, u32[]{:S(2)}) copy-start(f32[32,16,64]{2,1,0:T(8,128)S(1)} %get-tuple-element.25) | copy-start | bytes 393220
  61.1 29.0 %copy-start.4 = (f32[32,16,64]{2,1,0:T(8,128)}, f32[32,16,64]{2,1,0:T(8,128)S(1)}, u32[]{:S(2)}) copy-start(f32[32,16,64]{2,1,0:T(8,128)S(1)} %get-tuple-element.22) | copy-start | bytes 393220
  61.2 62.8 %copy-start.6 = (f32[32,16,64]{2,1,0:T(8,128)}, f32[32,16,64]{2,1,0:T(8,128)S(1)}, u32[]{:S(2)}) copy-start(f32[32,16,64]{2,1,0:T(8,128)S(1)} %get-tuple-element.23) | copy-start | bytes 393220
  61.3 28.8 %copy-start.8 = (f32[32,16,64]{2,1,0:T(8,128)}, f32[32,16,64]{2,1,0:T(8,128)S(1)}, u32[]{:S(2)}) copy-start(f32[32,16,64]{2,1,0:T(8,128)S(1)} %get-tuple-element.12) | copy-start | bytes 393220
  123.5 83.1 %copy-start.11 = (bf16[128,1024]{1,0:T(8,128)(2,1)S(1)}, bf16[128,1024]{1,0:T(8,128)(2,1)}, u32[]{:S(2)}) copy-start(bf16[128,1024]{1,0:T(8,128)(2,1)} %param.13) | copy-start | bytes 786436
  133.8 120.0 %reduce-scatter.5.cloned.1.call-start = ((), (), s32[]{:S(2)}) async-start(), calls=%async_computation.4 | async-start | bytes 3932160 | tf_op jit(solution)/shard_map/reduce_scatter | solution.py:93
  206.6 3.6 copy-start.17
  208.0 5.9 %copy-start.12 = (bf16[128,1024]{1,0:T(8,128)(2,1)}, bf16[128,1024]{1,0:T(8,128)(2,1)S(1)}, u32[]{:S(2)}) copy-start(bf16[128,1024]{1,0:T(8,128)(2,1)S(1)} %get-tuple-element.11) | copy-start | bytes 786436
  208.0 4.9 %copy-start.20 = (bf16[2,1024,1024]{2,1,0:T(8,128)(2,1)S(1)}, bf16[2,1024,1024]{2,1,0:T(8,128)(2,1)}, u32[]{:S(2)}) copy-start(bf16[2,1024,1024]{2,1,0:T(8,128)(2,1)} %param.18) | copy-start | bytes 12582916
  210.2 3.2 copy-start.22
  210.7 3.7 copy-start.23
  214.9 1.7 copy-start.1
  216.5 209.7 %all-reduce.7.cloned.1.call-start = ((), (), s32[]{:S(2)}) async-start(), calls=%async_computation.5 | async-start | bytes 1048576 | tf_op jit(solution)/shard_map/psum | solution.py:111
  256.2 28.7 %copy-start.3 = (f32[32,16,64]{2,1,0:T(8,128)S(1)}, f32[32,16,64]{2,1,0:T(8,128)}, u32[]{:S(2)}) copy-start(f32[32,16,64]{2,1,0:T(8,128)} %copy-done.2) | copy-start | bytes 393220
  256.2 28.7 %copy-start.5 = (f32[32,16,64]{2,1,0:T(8,128)S(1)}, f32[32,16,64]{2,1,0:T(8,128)}, u32[]{:S(2)}) copy-start(f32[32,16,64]{2,1,0:T(8,128)} %copy-done.4) | copy-start | bytes 393220
  256.2 28.7 %copy-start.7 = (f32[32,16,64]{2,1,0:T(8,128)S(1)}, f32[32,16,64]{2,1,0:T(8,128)}, u32[]{:S(2)}) copy-start(f32[32,16,64]{2,1,0:T(8,128)} %copy-done.6) | copy-start | bytes 393220
  256.2 28.7 %copy-start.9 = (f32[32,16,64]{2,1,0:T(8,128)S(1)}, f32[32,16,64]{2,1,0:T(8,128)}, u32[]{:S(2)}) copy-start(f32[32,16,64]{2,1,0:T(8,128)} %copy-done.8) | copy-start | bytes 393220
  353.5 72.8 %copy-start.13 = (bf16[128,1024]{1,0:T(8,128)(2,1)S(1)}, bf16[128,1024]{1,0:T(8,128)(2,1)}, u32[]{:S(2)}) copy-start(bf16[128,1024]{1,0:T(8,128)(2,1)} %copy-done.12) | copy-start | bytes 786436
Sparse Core Ops, SparseCore 0:
  18.2 40.6 reduce-scatter.2
  133.9 72.6 all-reduce.4
  216.7 37.0 reduce-scatter.4
  353.6 72.6 all-reduce.6
where the time goes:
time: 435 us
  waiting for transfers between devices  182 us (42%)
  matrix products  144 us (33%)
  other arithmetic  59.3 us (14%)
  blocking collectives  26 us (6%)
  between operations  15.1 us (3%)
  local copies, waits for them, and re-layouts  7.54 us (2%)
    psum x2, waiting for transfers between devices, per_device(): hidden = (hidden_wide + lax.psum(branch, 'tp')).astype(jnp.bfloat16)  121 us
    dot_general x2, matrix products, recurrent_mix_heads(): jnp.einsum('shvk,shk->shv', refreshed_state, receptance_rows, precision=l...  66.8 us
    reduce_scatter x2, waiting for transfers between devices, per_device(): lax.psum_scatter(partial_terms, 'dp', scatter_dimension=0, tiled=True)  61.4 us
    dot_general x2, matrix products, recurrent_mix_heads(): jnp.einsum('shvk,shk->shv', earlier_state, unit_key, precision=lax.Precis...  57.4 us
    add x1, other arithmetic, recurrent_mix_heads(): earlier_state * decay_factor[:, :, None, :]  24.9 us
    another operation x1, other arithmetic, per_device(): return (hidden, jnp.stack(new_states))  24.7 us
    unnamed x2, blocking collectives  14.4 us
    dot_general x12, matrix products, per_device(): jnp.dot(scaled_in, matrix, preferred_element_type=jnp.float32)  14.4 us
  transfers between devices with their start and end apart: 4, of which 4 were waited for; matrix products, arithmetic and copies ran while one was open for 6% of the time, Pallas kernels for 0%

commit v1 on v0

v1 whole, which is shorter than its diff:
```python
import functools

import jax
import jax.numpy as jnp
from jax import lax
from jax.experimental import pallas as pl
from jax.experimental.pallas import tpu as pltpu
from jax.sharding import PartitionSpec as P

HEAD_CHANNELS = 64
NT = (((1,), (1,)), ((), ()))
TN = (((0,), (0,)), ((), ()))
VMEM = pl.BlockSpec(memory_space=pltpu.VMEM)
ANY = pl.BlockSpec(memory_space=pl.ANY)


def remote(src, dst, send, recv, axis, to):
    return pltpu.make_async_remote_copy(
        src_ref=src,
        dst_ref=dst,
        send_sem=send,
        recv_sem=recv,
        device_id={axis: to},
        device_id_type=pl.DeviceIdType.MESH,
    )


def greet(sizes):
    barrier = pltpu.get_barrier_semaphore()
    count = 0
    for axis, size in sizes:
        me = lax.axis_index(axis)
        for step in range(1, size):
            pl.semaphore_signal(
                barrier,
                inc=1,
                device_id={axis: lax.rem(me + step, size)},
                device_id_type=pl.DeviceIdType.MESH,
            )
            count += 1
    pl.semaphore_wait(barrier, count)


def project_kernel(
    block, n, hidden, gain, w0, w1, w2, w3, w4, w5, out,
    wbuf, keep, send1, recv1, send2, recv2, squares, squares_in,
    wsem, s1, r1, s2, r2, sq_s, sq_r,
):
    weights = (w0, w1, w2, w3, w4, w5)
    batch, depth = hidden.shape
    rows = batch // n
    chips = n // 2
    loads = [
        pltpu.make_async_copy(w.at[block], wbuf.at[p], wsem.at[p]) for p, w in enumerate(weights)
    ]
    for load in loads:
        load.start()
    me = lax.axis_index("dp")
    core = lax.rem(me, 2)
    chip = lax.div(me, 2)
    partner = me + 1 - 2 * core
    wide = hidden[...].astype(jnp.float32)
    total = jnp.sum(wide * wide, axis=1, keepdims=True)
    squares[...] = jnp.broadcast_to(total, (batch, 128)).reshape(n, rows, 128)
    scaled = (wide * gain[block : block + 1, :]).astype(jnp.bfloat16)
    greet((("dp", n),))
    square_copies = []
    for j in range(1, n):
        to = lax.rem(me + j, n)
        copy = remote(squares.at[to], squares_in.at[j], sq_s.at[j], sq_r.at[j], "dp", to)
        copy.start()
        square_copies.append(copy)
    first = []
    second = []

    def cross(p):
        first[p].wait_recv()
        both = keep[p] + recv1[p].astype(jnp.float32)
        keep[p] = both
        send2[p] = both.astype(jnp.bfloat16)
        for j in range(1, chips):
            to = lax.rem(chip + j, chips)
            copy = remote(
                send2.at[p, to], recv2.at[p, j], s2.at[p, j], r2.at[p, j], "dp", 2 * to + core
            )
            copy.start()
            second.append((p, j, copy))

    for p in range(6):
        loads[p].wait()
        part = jnp.dot(scaled, wbuf[p], preferred_element_type=jnp.float32)
        part = part.reshape(chips, 2, rows, part.shape[1])
        even, odd = part[:, 0], part[:, 1]
        keep[p] = jnp.where(core == 0, even, odd)
        send1[p] = jnp.where(core == 0, odd, even).astype(jnp.bfloat16)
        copy = remote(send1.at[p], recv1.at[p], s1.at[p], r1.at[p], "dp", partner)
        copy.start()
        first.append(copy)
        if p >= 1:
            cross(p - 1)
    cross(5)
    mine = squares[me]
    for j, copy in enumerate(square_copies):
        copy.wait_recv()
        mine = mine + squares_in[j + 1]
    scale = lax.rsqrt(mine[:, :1] / (depth * n) + 1e-06)
    for p in range(6):
        value = keep[p, chip]
        for q, j, copy in second:
            if q == p:
                copy.wait_recv()
                value = value + recv2[p, j].astype(jnp.float32)
        out[p] = value * scale
    for copy in square_copies + first + [c for _, _, c in second]:
        copy.wait_send()


def project(block, n, hidden, gain, weights):
    batch, depth = hidden.shape
    width = weights[0].shape[2]
    rows, chips = batch // n, n // 2
    dma = pltpu.SemaphoreType.DMA
    return pl.pallas_call(
        functools.partial(project_kernel, block, n),
        out_shape=jax.ShapeDtypeStruct((6, rows, width), jnp.float32),
        in_specs=[VMEM, VMEM] + [ANY] * 6,
        out_specs=VMEM,
        scratch_shapes=[
            pltpu.VMEM((6, depth, width), jnp.bfloat16),
            pltpu.VMEM((6, chips, rows, width), jnp.float32),
            pltpu.VMEM((6, chips, rows, width), jnp.bfloat16),
            pltpu.VMEM((6, chips, rows, width), jnp.bfloat16),
            pltpu.VMEM((6, chips, rows, width), jnp.bfloat16),
            pltpu.VMEM((6, chips, rows, width), jnp.bfloat16),
            pltpu.VMEM((n, rows, 128), jnp.float32),
            pltpu.VMEM((n, rows, 128), jnp.float32),
            dma((6,)), dma((6,)), dma((6,)), dma((6, chips)), dma((6, chips)), dma((n,)), dma((n,)),
        ],
        compiler_params=pltpu.CompilerParams(collective_id=2 * block, has_side_effects=True),
        name=f"project{block}",
    )(hidden, gain, *weights)


def head_sums(value, ones):
    step = ones.shape[0]
    return jnp.concatenate(
        [
            jnp.dot(
                value[:, at : at + step],
                ones,
                preferred_element_type=jnp.float32,
                precision=lax.Precision.HIGHEST,
            )
            for at in range(0, value.shape[1], step)
        ],
        axis=1,
    )


def mix_kernel(block, steps, aliased, *refs):
    proj, floor, direct, norm_gain, state = refs[:5]
    out, mixed, ab, kr_heads, decay_heads, v_rows, krr_rows, y_rows = refs[5 + aliased :]
    at = pl.program_id(0)
    group, heads = state.shape[1:3]
    width = heads * HEAD_CHANNELS
    span = min(128, width)
    ones = (
        lax.broadcasted_iota(jnp.int32, (span, span), 0) // HEAD_CHANNELS
        == lax.broadcasted_iota(jnp.int32, (span, span), 1) // HEAD_CHANNELS
    ).astype(jnp.float32)

    @pl.when(at == 0)
    def _():
        r, k, v, pd, pa = proj[0], proj[1], proj[2], proj[3], proj[4]
        decay = jnp.exp(-jnp.exp(-jax.nn.softplus(-(floor[block : block + 1, :] + pd)) - 0.5))
        kr = k * jax.nn.sigmoid(pa)
        a = k / (head_sums(k * k, ones) + 1e-06)
        b = decay * r
        v_rows[...] = v
        krr_rows[...] = head_sums(kr * r, ones)
        for h in range(heads):
            cut = slice(h * HEAD_CHANNELS, (h + 1) * HEAD_CHANNELS)
            ab[:, h, :] = a[:, cut]
            ab[:, heads + h, :] = b[:, cut]
            kr_heads[:, h, :] = kr[:, cut]
            decay_heads[:, h, :] = decay[:, cut]

    own = (
        lax.broadcasted_iota(jnp.int32, (heads, width), 0)
        == lax.broadcasted_iota(jnp.int32, (heads, width), 1) // HEAD_CHANNELS
    )
    for s in range(group):
        row = at * group + s
        flat = state[0, s].reshape(width, HEAD_CHANNELS)
        both = lax.dot_general(
            ab[row].astype(jnp.bfloat16),
            flat.astype(jnp.bfloat16),
            NT,
            preferred_element_type=jnp.float32,
        )
        removed = jnp.sum(jnp.where(own, both[:heads], 0.0), axis=0, keepdims=True)
        kept = jnp.sum(jnp.where(own, both[heads:], 0.0), axis=0, keepdims=True)
        added = v_rows[pl.ds(row, 1), :] - removed
        y_rows[pl.ds(row, 1), :] = kept + added * krr_rows[pl.ds(row, 1), :]
        spread = jnp.where(own, added, 0.0).astype(jnp.bfloat16)
        outer = lax.dot_general(
            spread, kr_heads[row].astype(jnp.bfloat16), TN, preferred_element_type=jnp.float32
        )
        old = flat.reshape(heads, HEAD_CHANNELS, HEAD_CHANNELS)
        out[0, s] = old * decay_heads[row][:, None, :] + outer.reshape(old.shape)

    @pl.when(at == steps - 1)
    def _():
        y = y_rows[...]
        centred = y - head_sums(y, ones) / HEAD_CHANNELS
        var = head_sums(centred * centred, ones) / HEAD_CHANNELS
        r, k, v, pa, pg = proj[0], proj[1], proj[2], proj[4], proj[5]
        kr = k * jax.nn.sigmoid(pa)
        term = head_sums(r * kr * direct[block : block + 1, :], ones) * v
        normed = centred * lax.rsqrt(var + 0.00064) * norm_gain[block : block + 1, :]
        mixed[...] = ((normed + term) * jax.nn.sigmoid(pg)).astype(jnp.bfloat16)


def mix(block, proj, floor, direct, norm_gain, state, earlier):
    blocks, rows, heads = state.shape[:3]
    width = heads * HEAD_CHANNELS
    group = 4
    steps = rows // group
    aliased = earlier is not None
    tile = pl.BlockSpec(
        (1, group, heads, HEAD_CHANNELS, HEAD_CHANNELS), lambda i: (block, i, 0, 0, 0)
    )
    whole = lambda shape: pl.BlockSpec(shape, lambda i: (0,) * len(shape))
    f32 = jnp.float32
    return pl.pallas_call(
        functools.partial(mix_kernel, block, steps, int(aliased)),
        grid=(steps,),
        out_shape=(
            jax.ShapeDtypeStruct(state.shape, f32),
            jax.ShapeDtypeStruct((rows, width), jnp.bfloat16),
        ),
        in_specs=[whole(proj.shape)] + [whole((blocks, width))] * 3 + [tile] + [ANY] * aliased,
        out_specs=(tile, whole((rows, width))),
        scratch_shapes=[
            pltpu.VMEM((rows, 2 * heads, HEAD_CHANNELS), f32),
            pltpu.VMEM((rows, heads, HEAD_CHANNELS), f32),
            pltpu.VMEM((rows, heads, HEAD_CHANNELS), f32),
            pltpu.VMEM((rows, width), f32),
            pltpu.VMEM((rows, width), f32),
            pltpu.VMEM((rows, width), f32),
        ],
        input_output_aliases={5: 0} if aliased else {},
        compiler_params=pltpu.CompilerParams(dimension_semantics=("arbitrary",)),
        name=f"mix{block}",
    )(proj, floor, direct, norm_gain, state, *([earlier] if aliased else []))


def merge_kernel(
    block, n, nt, mixed, hidden, weight, out,
    wbuf, gathered, partial, send, recv, fresh, landed, wsem, gs, gr, rs_s, rs_r, ag_s, ag_r,
):
    load = pltpu.make_async_copy(weight.at[block], wbuf, wsem)
    load.start()
    batch, cols = hidden.shape
    rows, slab = batch // n, batch // nt
    me, rank = lax.axis_index("dp"), lax.axis_index("tp")
    greet((("dp", n), ("tp", nt)))
    gathers = []
    for j in range(1, n):
        to = lax.rem(me + j, n)
        gathers.append(remote(mixed, gathered.at[me], gs.at[j], gr.at[j], "dp", to))
    for copy in gathers:
        copy.start()
    gathered[me] = mixed[...]
    load.wait()
    for copy in gathers:
        copy.wait_recv()
    product = jnp.dot(
        gathered[...].reshape(batch, mixed.shape[1]), wbuf[...], preferred_element_type=jnp.float32
    ).reshape(nt, slab, cols)
    partial[...] = product
    send[...] = product.astype(jnp.bfloat16)
    scatters = []
    for j in range(1, nt):
        to = lax.rem(rank + j, nt)
        scatters.append(remote(send.at[to], recv.at[j], rs_s.at[j], rs_r.at[j], "tp", to))
    for copy in scatters:
        copy.start()
    start = pl.multiple_of(rank * slab, slab)
    value = hidden[pl.ds(start, slab), :].astype(jnp.float32) + partial[rank]
    for j, copy in enumerate(scatters):
        copy.wait_recv()
        value = value + recv[j + 1].astype(jnp.float32)
    fresh[...] = value.astype(jnp.bfloat16)
    spreads = []
    for j in range(1, nt):
        to = lax.rem(rank + j, nt)
        spreads.append(remote(fresh, landed.at[rank], ag_s.at[j], ag_r.at[j], "tp", to))
    for copy in spreads:
        copy.start()
    landed[rank] = value.astype(jnp.bfloat16)
    for copy in spreads:
        copy.wait_recv()
    out[...] = landed[...].reshape(batch, cols)
    for copy in gathers + scatters + spreads:
        copy.wait_send()


def merge(block, n, nt, mixed, hidden, weight):
    batch, cols = hidden.shape
    rows, width = mixed.shape
    slab = batch // nt
    if slab % 16:
        branch = jnp.dot(
            lax.all_gather(mixed, "dp", axis=0, tiled=True),
            weight[block],
            preferred_element_type=jnp.float32,
        )
        return (hidden.astype(jnp.float32) + lax.psum(branch, "tp")).astype(jnp.bfloat16)
    dma = pltpu.SemaphoreType.DMA
    bf16 = jnp.bfloat16
    return pl.pallas_call(
        functools.partial(merge_kernel, block, n, nt),
        out_shape=jax.ShapeDtypeStruct((batch, cols), bf16),
        in_specs=[VMEM, VMEM, ANY],
        out_specs=VMEM,
        scratch_shapes=[
            pltpu.VMEM((width, cols), bf16),
            pltpu.VMEM((n, rows, width), bf16),
            pltpu.VMEM((nt, slab, cols), jnp.float32),
            pltpu.VMEM((nt, slab, cols), bf16),
            pltpu.VMEM((nt, slab, cols), bf16),
            pltpu.VMEM((slab, cols), bf16),
            pltpu.VMEM((nt, slab, cols), bf16),
            dma, dma((n,)), dma((n,)), dma((nt,)), dma((nt,)), dma((nt,)), dma((nt,)),
        ],
        compiler_params=pltpu.CompilerParams(collective_id=2 * block + 1, has_side_effects=True),
        name=f"merge{block}",
    )(mixed, hidden, weight)


def solution(mesh):
    n, nt = mesh.shape["dp"], mesh.shape["tp"]

    def per_device(token, gain, wr, wk, wv, wd, wa, wg, floor, direct, norm_gain, wo, state):
        hidden, states = token, None
        for block in range(state.shape[0]):
            proj = project(block, n, hidden, gain, (wr, wk, wv, wd, wa, wg))
            states, mixed = mix(block, proj, floor, direct, norm_gain, state, states)
            hidden = merge(block, n, nt, mixed, hidden, wo)
        return hidden, states

    return jax.shard_map(
        per_device,
        mesh=mesh,
        in_specs=(
            P(None, "dp"),
            P(None, "dp"),
            *[P(None, "dp", "tp")] * 6,
            *[P(None, "tp")] * 3,
            P(None, "tp", "dp"),
            P(None, "dp", "tp", None, None),
        ),
        out_specs=(P(None, "dp"), P(None, "dp", "tp", None, None)),
        check_vma=False,
    )
```

time: 435 us -> 125 us (0.29)
  waiting for transfers between devices: 182 us -> 0 us
  matrix products: 144 us -> 0 us
  Pallas kernels: 0 us -> 122 us
  other arithmetic: 59.3 us -> 0 us
  blocking collectives: 26 us -> 0 us
  between operations: 15.1 us -> 0.66 us
  local copies, waits for them, and re-layouts: 7.54 us -> 1.67 us
    dot_general x18 -> x0, matrix products: 144 us -> none  [the longest x2 66.8 us: recurrent_mix_heads(): jnp.einsum('shvk,shk->shv', refreshed_state, receptance_rows, precision=l...]
    pallas_call x0 -> x6, Pallas kernels: none -> 122 us  [the longest x2 46.8 us: merge(): pl.pallas_call(functools.partial(merge_kernel, block, n, nt), out_shape=j...]
    psum x2 -> x0, waiting for transfers between devices: 121 us -> none  [per_device(): hidden = (hidden_wide + lax.psum(branch, 'tp')).astype(jnp.bfloat16)]
    reduce_scatter x2 -> x0, waiting for transfers between devices: 61.4 us -> none  [per_device(): lax.psum_scatter(partial_terms, 'dp', scatter_dimension=0, tiled=True)]
    add x1 -> x0, other arithmetic: 24.9 us -> none  [recurrent_mix_heads(): earlier_state * decay_factor[:, :, None, :]]
    another operation x1 -> x0, other arithmetic: 24.7 us -> none  [per_device(): return (hidden, jnp.stack(new_states))]
    unnamed x2 -> x0, blocking collectives: 14.4 us -> none
    all_gather x2 -> x0, blocking collectives: 11.6 us -> none  [per_device(): lax.all_gather(mixer_output, 'dp', axis=0, tiled=True)]
  transfers between devices with their start and end apart: 4 -> 0, of which waited for: 4 -> 0; matrix products, arithmetic and copies ran while one was open for 6% -> 0% of each run, Pallas kernels for 0% -> 0%
where the time goes in v1:
time: 125 us; the launch traced here: 124 us
  Pallas kernels  122 us (98%)
  local copies, waits for them, and re-layouts  1.67 us (1%)
    pallas_call x2, Pallas kernels, merge(): pl.pallas_call(functools.partial(merge_kernel, block, n, nt), out_shape=j...  46.8 us
    pallas_call x2, Pallas kernels, mix(): pl.pallas_call(functools.partial(mix_kernel, block, steps, int(aliased)),...  40.5 us
    pallas_call x2, Pallas kernels, project(): pl.pallas_call(functools.partial(project_kernel, block, n), out_shape=jax...  34.8 us

profile of v1, /device:TPU:0, one launch (start us, length us, event | category | flops | bytes accessed | tf_op | source)
XLA Modules:
  0.0 124.4 jit_solution(16342415375747408940)
XLA Ops:
  0.6 18.0 %project0.1.refs_0_ = f32[6,32,1024]{2,1,0:T(8,128)} custom-call(bf16[128,1024]{1,0:T(8,128)(2,1)} %hidden.3, f32[2,1024]{1,0:T(2,128)} %gain.3, bf16[2,1024,1024]{2,1,0:T(8,128)(2,1)} %w0.3, bf16[2,1024,1024]{2,1,0:T(8,128)(2,1)} %w1.3, bf16[2,1024,1024]{2,1,0:T(8,128)(2,1)} %w2.3, bf16[2,1024,1024]{2,1,0:T(8,128)(2,1)} %w3.3, bf16[2,1024,1024]{2,1,0:T(8,128)(2,1)} %w4.3, ...), custom_call_target="tpu_custom_call" | custom-call | tf_op jit(solution)/shard_map/project0/pallas_call | solution.py:123
  18.6 20.3 %mix0.1 = (f32[2,32,16,64,64]{4,3,2,1,0:T(8,128)}, bf16[32,1024]{1,0:T(8,128)(2,1)}) custom-call(f32[6,32,1024]{2,1,0:T(8,128)} %project0.1.refs_0_, f32[2,1024]{1,0:T(2,128)} %refs_1_.3, f32[2,1024]{1,0:T(2,128)} %refs_2_.3, f32[2,1024]{1,0:T(2,128)} %refs_3_.3, f32[2,32,16,64,64]{4,3,2,1,0:T(8,128)} %refs_4_.3), custom_call_target="tpu_custom_call" | custom-call | tf_op jit(solution)/shard_map/mix0/pallas_call | solution.py:235
  39.0 23.4 %merge0.1.hidden = bf16[128,1024]{1,0:T(8,128)(2,1)} custom-call(bf16[32,1024]{1,0:T(8,128)(2,1)} %get-tuple-element.6.mixed, bf16[128,1024]{1,0:T(8,128)(2,1)} %hidden.3, bf16[2,1024,1024]{2,1,0:T(8,128)(2,1)} %weight.3), custom_call_target="tpu_custom_call" | custom-call | tf_op jit(solution)/shard_map/merge0/pallas_call | solution.py:322
  62.3 16.8 %project1.1.refs_0_ = f32[6,32,1024]{2,1,0:T(8,128)} custom-call(bf16[128,1024]{1,0:T(8,128)(2,1)} %merge0.1.hidden, f32[2,1024]{1,0:T(2,128)} %gain.3, bf16[2,1024,1024]{2,1,0:T(8,128)(2,1)} %w0.3, bf16[2,1024,1024]{2,1,0:T(8,128)(2,1)} %w1.3, bf16[2,1024,1024]{2,1,0:T(8,128)(2,1)} %w2.3, bf16[2,1024,1024]{2,1,0:T(8,128)(2,1)} %w3.3, ...), custom_call_target="tpu_custom_call" | custom-call | tf_op jit(solution)/shard_map/project1/pallas_call | solution.py:123
  79.1 20.2 %mix1.1 = (f32[2,32,16,64,64]{4,3,2,1,0:T(8,128)}, bf16[32,1024]{1,0:T(8,128)(2,1)}) custom-call(f32[6,32,1024]{2,1,0:T(8,128)} %project1.1.refs_0_, f32[2,1024]{1,0:T(2,128)} %refs_1_.3, f32[2,1024]{1,0:T(2,128)} %refs_2_.3, f32[2,1024]{1,0:T(2,128)} %refs_3_.3, f32[2,32,16,64,64]{4,3,2,1,0:T(8,128)} %refs_4_.3, ...), custom_call_target="tpu_custom_call", output_to_operand_aliasing={{0}: (5, {})} | custom-call | tf_op jit(solution)/shard_map/mix1/pallas_call | solution.py:235
  99.3 23.5 %merge1.1 = bf16[128,1024]{1,0:T(8,128)(2,1)} custom-call(bf16[32,1024]{1,0:T(8,128)(2,1)} %get-tuple-element.8.mixed, bf16[128,1024]{1,0:T(8,128)(2,1)} %merge0.1.hidden, bf16[2,1024,1024]{2,1,0:T(8,128)(2,1)} %weight.3), custom_call_target="tpu_custom_call" | custom-call | tf_op jit(solution)/shard_map/merge1/pallas_call | solution.py:322
  122.8 1.7 %copy.18 = bf16[128,1024]{1,0:T(8,128)(2,1)} copy(bf16[128,1024]{1,0:T(8,128)(2,1)} %merge1.1) | data formatting | bytes 524288
